TPU v7x, 128 devices: a whole 4x4x4 slice. The times are simulated.
128 devices in a mesh: sp: 16 (over z, y), tp: 8 (over x, core).
Axes of the slice: x: 4, y: 4, z: 4, core: 2. Of those that a mesh axis runs over, the one named last changes fastest.
Arguments:
- queries: bfloat16 [12288, 2048], P('sp', 'tp'), may hold values from -11 to 11
- key_rows: bfloat16 [12288, 2048], P('sp', 'tp'), may hold values from -4.5 to 4.5
- value_rows: bfloat16 [12288, 2048], P('sp', 'tp'), may hold values from -6 to 6
- log_forget: float32 [12288, 32], P('sp', 'tp'), may hold values from -1477.56 to 0, as said below
- stream_in: bfloat16 [12288, 2048], P('sp'), may hold values from -6 to 6
- out_weight: bfloat16 [2048, 2048], P('tp'), may hold values from -0.52734375 to 0.52734375
- mix_gain: float32 [2048], replicated, may hold values from 0.1 to 1.9
- mix_bias: float32 [2048], replicated, may hold values from -3 to 3
- gate_weight: bfloat16 [2048, 5632], P('sp', 'tp'), may hold values from -0.125 to 0.125
- up_weight: bfloat16 [2048, 5632], P('sp', 'tp'), may hold values from -0.125 to 0.125
- down_weight: bfloat16 [5632, 2048], P('tp', 'sp'), may hold values from -0.15917969 to 0.15917969
- ffn_gain: float32 [2048], replicated, may hold values from 0.1 to 1.9
- ffn_bias: float32 [2048], replicated, may hold values from -3 to 3
Outputs:
- layer_out: bfloat16 [12288, 2048], P(('sp', 'tp'))
Inputs may be any that keep to these rules, and one draw needn't show every extreme that they name: `log_forget`: each column never rises along the positions.
All inputs are finite; a program needn't handle non-finite values.
Results may differ from a plain program's by a relative error of at most 0.015.
Values may be sent and summed in bfloat16 or wider, within the bound.
A program may use at most 128 MiB of HBM per device.

v0:
```python
import jax
import jax.numpy as jnp
from jax import lax
from jax.sharding import PartitionSpec as P

ALPHA = 8.0**0.25
EPSILON = 1e-05


def laid_out(pieces, dim):
    lengths = list(pieces.shape[1:])
    lengths[dim] *= pieces.shape[0]
    return jnp.moveaxis(pieces, 0, dim).reshape(lengths)


def from_everyone(value, axis):
    copies = jnp.broadcast_to(value, (lax.axis_size(axis), *value.shape))
    return lax.all_to_all(copies, axis, split_axis=0, concat_axis=0, tiled=True)


def gathered_copies(value, axis, dim):
    return laid_out(from_everyone(value, axis), dim)


def in_one_piece(arrays, axis, dim, along):
    ends, at = ([], 0)
    for a in arrays[:-1]:
        at += a.shape[along]
        ends.append(at)
    both = jnp.concatenate(arrays, axis=along)
    return tuple(jnp.split(lax.all_gather(both, axis, axis=dim, tiled=True), ends, axis=along))


def in_blocks(value, dim, count):
    before, after = (value.shape[:dim], value.shape[dim + 1 :])
    return jnp.moveaxis(value.reshape(*before, count, -1, *after), dim, 0)


def sum_at_owner(value, axis, dim):
    pieces = in_blocks(value, dim, lax.axis_size(axis))
    arrived = lax.all_to_all(pieces, axis, split_axis=0, concat_axis=0, tiled=True)
    return arrived.astype(jnp.float32).sum(axis=0)


def layer_norm(matrix, norm_gain, norm_shift):
    centred = matrix - jnp.mean(matrix, axis=-1, keepdims=True)
    spread = jnp.mean(centred * centred, axis=-1, keepdims=True)
    return centred * lax.rsqrt(spread + EPSILON) * norm_gain + norm_shift


def attend(queries, key_rows, value_rows, log_forget):
    length, row_width = queries.shape
    head_count = log_forget.shape[1]
    head_dim = row_width // head_count
    score_scale = head_dim ** (-0.5)
    first_pos = lax.axis_index("sp") * length
    last_pos = first_pos + length
    query_heads = queries.reshape(length, head_count, head_dim)
    query_gates = log_forget.T
    query_pos = first_pos + jnp.arange(length, dtype=jnp.int32)
    gates_all = gathered_copies(log_forget, "sp", 0)
    initial = (
        jnp.full((head_count, length), -1e30, jnp.float32),
        jnp.zeros((head_count, length), jnp.float32),
        jnp.zeros((length, head_count, head_dim), jnp.float32),
    )
    running = initial
    key_piece, value_piece = in_one_piece((key_rows, value_rows), "sp", 0, 1)
    piece_len = key_piece.shape[0]
    shards = piece_len // length
    group_size = max(
        [
            count_try
            for count_try in range(1, shards + 1)
            if shards % count_try == 0 and count_try * length <= max(length, 512)
        ]
    )
    block_len = group_size * length
    blocks = piece_len // block_len
    key_blocks = key_piece.reshape(blocks, block_len, head_count, head_dim)
    value_blocks = value_piece.reshape(blocks, block_len, head_count, head_dim)
    gate_blocks = gates_all.reshape(blocks, block_len, head_count)
    block_starts = block_len * jnp.arange(blocks, dtype=jnp.int32)

    def one_block(running_state, packed):
        key_block, value_block, gate_block, block_start = packed

        def compute(state_in):
            highest, totals, weighted = state_in
            scores = (
                jnp.einsum(
                    "qhd,khd->hqk", query_heads, key_block, preferred_element_type=jnp.float32
                )
                * score_scale
            )
            scores = scores + query_gates[:, :, None] - gate_block.T[:, None, :]
            key_pos = block_start + jnp.arange(block_len, dtype=jnp.int32)
            allowed = (key_pos[None, :] <= query_pos[:, None])[None]
            masked = jnp.where(allowed, scores, -1e30)
            new_high = jnp.maximum(highest, jnp.max(masked, axis=2))
            weights = jnp.where(allowed, jnp.exp(masked - new_high[:, :, None]), 0.0)
            factor = jnp.exp(highest - new_high)
            totals = totals * factor + jnp.sum(weights, axis=2)
            weighted = weighted * factor.T[:, :, None] + jnp.einsum(
                "hqk,khd->qhd",
                weights.astype(jnp.bfloat16),
                value_block,
                preferred_element_type=jnp.float32,
            )
            return (new_high, totals, weighted)

        def keep_state(state_in):
            return state_in

        return (lax.cond(block_start < last_pos, compute, keep_state, running_state), None)

    running, unused = lax.scan(
        one_block, running, (key_blocks, value_blocks, gate_blocks, block_starts)
    )
    highest, totals, weighted = running
    return (weighted / totals.T[:, :, None]).reshape(length, row_width).astype(jnp.bfloat16)


def body(
    queries,
    key_rows,
    value_rows,
    log_forget,
    stream_in,
    out_weight,
    mix_gain,
    mix_bias,
    gate_weight,
    up_weight,
    down_weight,
    ffn_gain,
    ffn_bias,
):
    attended = attend(queries, key_rows, value_rows, log_forget)
    length = attended.shape[0]
    own_rows = length // lax.axis_size("tp")
    offset = lax.axis_index("tp") * own_rows
    summed = sum_at_owner(
        jnp.dot(attended, out_weight, preferred_element_type=jnp.float32).astype(jnp.bfloat16),
        "tp",
        0,
    )
    mix_out = lax.optimization_barrier(summed.astype(jnp.bfloat16)).astype(jnp.float32)
    stream_own = lax.dynamic_slice_in_dim(stream_in, offset, own_rows, 0)
    normed = layer_norm(
        ALPHA * stream_own.astype(jnp.float32) + mix_out, mix_gain, mix_bias
    ).astype(jnp.bfloat16)
    gathered = lax.all_gather(normed, "tp", axis=0, tiled=True)
    pieces = in_one_piece((gate_weight, up_weight), "sp", 0, 1)
    gate_part = jnp.dot(gathered, pieces[0], preferred_element_type=jnp.float32)
    up_part = jnp.dot(gathered, pieces[1], preferred_element_type=jnp.float32)
    hidden = (jax.nn.silu(gate_part) * up_part).astype(jnp.bfloat16)
    partial_terms = jnp.dot(
        hidden,
        lax.all_gather(down_weight, "sp", axis=1, tiled=True),
        preferred_element_type=jnp.float32,
    )
    lowered = lax.psum_scatter(
        partial_terms.astype(jnp.bfloat16), "tp", scatter_dimension=0, tiled=True
    ).astype(jnp.float32)
    lowered = lax.optimization_barrier(lowered.astype(jnp.bfloat16)).astype(jnp.float32)
    result = layer_norm(ALPHA * normed.astype(jnp.float32) + lowered, ffn_gain, ffn_bias)
    return result.astype(jnp.bfloat16)


def solution(mesh):
    placed = (
        P("sp", "tp"),
        P("sp", "tp"),
        P("sp", "tp"),
        P("sp", "tp"),
        P("sp", None),
        P("tp", None),
        P(),
        P(),
        P("sp", "tp"),
        P("sp", "tp"),
        P("tp", "sp"),
        P(),
        P(),
    )
    return jax.shard_map(
        body, mesh=mesh, in_specs=placed, out_specs=P(("sp", "tp"), None), check_vma=False
    )
```

profile of v0, /device:TPU:0, one launch (start us, length us, event | category | flops | bytes accessed | tf_op | source)
XLA Modules:
  0.0 604.3 jit_solution(4880820120093457124)
XLA Ops:
  6.5 2.2 pad_maximum_fusion
  8.8 1.8 pad_maximum_fusion.1
  10.6 1.4 broadcast_in_dim.56
  12.0 8.2 %all-to-all-start = ((f32[16,768,4]{1,2,0:T(4,128)}), f32[16,768,4]{1,2,0:T(4,128)S(1)}, u32[]{:S(2)}, u32[]{:S(2)}) async-start(f32[16,768,4]{1,2,0:T(4,128)} %broadcast_in_dim.56), calls=%async_computation | async-start | bytes 393216 | tf_op jit(solution)/shard_map/all_to_all | solution.py:18
  20.2 1.2 copy.18
  21.4 80.5 %all-gather.5.cloned.1.call-done = bf16[12288,512]{1,0:T(8,128)(2,1)} async-done(((bf16[768,512]{1,0:T(8,128)(2,1)}), bf16[12288,512]{1,0:T(8,128)(2,1)}) %all-gather.5.cloned.1.call-update) | async-done | bytes 12582928 | tf_op jit(solution)/shard_map/all_gather | solution.py:31
  101.9 10.1 %fusion.36 = (bf16[12288,256]{1,0:T(8,128)(2,1)}, bf16[12288,256]{1,0:T(8,128)(2,1)}) fusion(bf16[12288,512]{1,0:T(8,128)(2,1)} %all-gather.5.cloned.1.call-done), kind=kLoop, calls=%fused_computation.51 | loop fusion | bytes 25165824 | tf_op jit(solution)/shard_map/split | solution.py:31
  112.0 18.8 %reshape.82 = bf16[16,768,4,64]{3,2,1,0:T(4,128)(2,1)} reshape(bf16[12288,256]{1,0:T(8,128)(2,1)} %get-tuple-element.249) | data formatting | bytes 12582912 | tf_op jit(solution)/shard_map/reshape | solution.py:80
  130.8 18.1 %copy.20 = bf16[16,768,4,64]{1,3,2,0:T(8,128)(2,1)} copy(bf16[16,768,4,64]{3,2,1,0:T(4,128)(2,1)} %reshape.82) | data formatting | bytes 12582912
  148.9 18.8 %reshape.83 = bf16[16,768,4,64]{3,2,1,0:T(4,128)(2,1)} reshape(bf16[12288,256]{1,0:T(8,128)(2,1)} %get-tuple-element.248) | data formatting | bytes 12582912 | tf_op jit(solution)/shard_map/reshape | solution.py:81
  167.6 18.1 %copy.21 = bf16[16,768,4,64]{1,3,2,0:T(8,128)(2,1)} copy(bf16[16,768,4,64]{3,2,1,0:T(4,128)(2,1)} %reshape.83) | data formatting | bytes 12582912
  185.8 33.5 %while.15 = (s32[]{:T(128)}, f32[4,768]{1,0:T(4,128)S(1)}, f32[4,768]{1,0:T(4,128)S(1)}, f32[768,4,64]{0,2,1:T(8,128)S(1)}, s32[16]{0:T(128)S(1)}, /*index=5*/s3...) while((s32[]{:T(128)}, f32[4,768]{1,0:T(4,128)S(1)}, ...), condition=%wide.region_5.6_spmd.clone, body=%wide.region_0.5_spmd.clone.sunk | while | flops 649800192 | bytes 33738040 | solution.py:117
  187.1 13.1 %conditional.3 = ((f32[4,768]{1,0:T(4,128)S(1)}, f32[4,768]{1,0:T(4,128)S(1)}, f32[768,4,64]{0,2,1:T(8,128)S(1)})) conditional(s32[]{:T(128)} %convert_element_type.100, (f32[4,768]{1,0:T(4,128)S(1)}, f32[4,768]{1,0:T(4,128)S(1)}, f32[768,4,64]{0,2,1:T(8,128)S(1)}) %tuple.41, (s32[]{:T(128)}, s32[]{:T(128)}, bf16[16,768,4,64]{1,3,2,0:T(8,128)(2,1)}, ...), branch_computations={%region_1.1_spmd, %region_2.4_spmd} | conditional | flops 649800192 | bytes 33734700 | solution.py:115
  187.1 0.7 iota_add_fusion
  188.2 3.9 fusion.4
  192.0 4.6 fusion.11
  196.6 3.5 fusion.3
  219.4 2.7 convolution_convert_fusion.1
  222.1 4.6 all-to-all-start.1
  226.9 38.2 %all-to-all-done.1 = bf16[8,96,2048]{2,1,0:T(8,128)(2,1)} async-done(((bf16[8,96,2048]{2,1,0:T(8,128)(2,1)}), bf16[8,96,2048]{2,1,0:T(8,128)(2,1)}, u32[]{:S(2)}, u32[]{:S(2)}) %all-to-all-start.1) | async-done | bytes 3145760 | tf_op jit(solution)/shard_map/all_to_all | solution.py:41
  265.1 2.5 reduce_sum.59
  267.6 1.2 fusion.33
  268.8 1.3 multiply_reduce_fusion.1
  270.2 2.0 add_convert_fusion.1
  272.8 220.0 %all-gather.7.cloned.1.call-done = bf16[768,2048]{1,0:T(8,128)(2,1)} async-done(((bf16[96,2048]{1,0:T(8,128)(2,1)}), bf16[768,2048]{1,0:T(8,128)(2,1)}) %all-gather.7.cloned.1.call-update) | async-done | bytes 3145744 | tf_op jit(solution)/shard_map/all_gather | solution.py:153
  492.8 6.5 %fusion.27 = f32[768,704]{0,1:T(8,128)} fusion(bf16[768,2048]{1,0:T(8,128)(2,1)} %all-gather.7.cloned.1.call-done, bf16[2048,1408]{0,1:T(8,128)(2,1)} %all-gather.9.cloned.1.call-done), kind=kOutput, calls=%fused_computation.31 | convolution fusion | flops 2214592512 | bytes 8192000 | tf_op jit(solution)/shard_map/dot_general | solution.py:155
  499.3 46.2 %all-gather.11.cloned.1.call-done = bf16[704,2048]{1,0:T(8,128)(2,1)} async-done(((bf16[704,128]{1,0:T(8,128)(2,1)}), bf16[704,2048]{1,0:T(8,128)(2,1)}) %all-gather.11.cloned.1.call-update) | async-done | bytes 2883600 | tf_op jit(solution)/shard_map/all_gather | solution.py:160
  545.5 12.4 %convolution_convert_fusion = bf16[768,2048]{1,0:T(8,128)(2,1)} fusion(bf16[704,2048]{1,0:T(8,128)(2,1)} %all-gather.11.cloned.1.call-done, f32[768,704]{0,1:T(8,128)} %fusion.27, bf16[768,2048]{1,0:T(8,128)(2,1)} %all-gather.7.cloned.1.call-done, bf16[2048,1408]{0,1:T(8,128)(2,1)} %all-gather.9.cloned.1.call-done), kind=kOutput, calls=%fused_computation.27 | convolution fusion | flops 4434001920 | bytes 14221312 | tf_op jit(solution)/shard_map/dot_general | solution.py:158
  557.9 35.3 %reduce-scatter.2.cloned.1.call-done = bf16[96,2048]{1,0:T(8,128)(2,1)} async-done(((bf16[768,2048]{1,0:T(8,128)(2,1)}), bf16[96,2048]{1,0:T(8,128)(2,1)}) %reduce-scatter.2.cloned.1.call-update) | async-done | bytes 393232 | tf_op jit(solution)/shard_map/reduce_scatter | solution.py:163
  593.2 1.2 fusion.34
  594.4 1.3 multiply_reduce_fusion
  595.7 2.0 add_convert_fusion
  (87 shorter events, 11.2 us)
Async XLA Ops:
  6.5 212.9 %copy-start = (bf16[256,2048]{1,0:T(8,128)(2,1)S(1)}, bf16[256,2048]{1,0:T(8,128)(2,1)}, u32[]{:S(2)}) copy-start(bf16[256,2048]{1,0:T(8,128)(2,1)} %param.22) | copy-start | bytes 3145732
  6.5 95.4 %all-gather.5.cloned.1.call-start = ((), (), s32[]{:S(2)}) async-start(), calls=%async_computation.3 | async-start | bytes 13369344 | tf_op jit(solution)/shard_map/all_gather | solution.py:31
  8.8 264.1 %all-gather.9.cloned.1.call-start = ((), (), s32[]{:S(2)}) async-start(), calls=%async_computation.5 | async-start | bytes 6127616 | tf_op jit(solution)/shard_map/all_gather | solution.py:31
  12.0 173.7 %all-to-all-start = ((f32[16,768,4]{1,2,0:T(4,128)}), f32[16,768,4]{1,2,0:T(4,128)S(1)}, u32[]{:S(2)}, u32[]{:S(2)}) async-start(f32[16,768,4]{1,2,0:T(4,128)} %broadcast_in_dim.56), calls=%async_computation | async-start | bytes 393216 | tf_op jit(solution)/shard_map/all_to_all | solution.py:18
  167.6 18.2 %copy-start.2 = (f32[768,4]{0,1:T(4,128)S(1)}, f32[768,4]{0,1:T(4,128)}, u32[]{:S(2)}) copy-start(f32[768,4]{0,1:T(4,128)} %param.20) | copy-start | bytes 36868
  222.1 48.0 %copy-start.3 = (f32[2048]{0:T(1024)S(1)}, f32[2048]{0:T(1024)}, u32[]{:S(2)}) copy-start(f32[2048]{0:T(1024)} %param.24) | copy-start | bytes 24580
  222.1 48.0 %copy-start.4 = (f32[2048]{0:T(1024)S(1)}, f32[2048]{0:T(1024)}, u32[]{:S(2)}) copy-start(f32[2048]{0:T(1024)} %param.23) | copy-start | bytes 24580
  222.1 43.0 %all-to-all-start.1 = ((bf16[8,96,2048]{2,1,0:T(8,128)(2,1)}), bf16[8,96,2048]{2,1,0:T(8,128)(2,1)}, u32[]{:S(2)}, u32[]{:S(2)}) async-start(bf16[8,96,2048]{2,1,0:T(8,128)(2,1)} %bitcast.45), calls=%async_computation.1 | async-start | bytes 6291456 | tf_op jit(solution)/shard_map/all_to_all | solution.py:41
  226.7 266.1 %all-gather.7.cloned.1.call-start = ((), (), s32[]{:S(2)}) async-start(), calls=%async_computation.4 | async-start | bytes 3538944 | tf_op jit(solution)/shard_map/all_gather | solution.py:153
  272.2 273.3 %all-gather.11.cloned.1.call-start = ((), (), s32[]{:S(2)}) async-start(), calls=%async_computation.6 | async-start | bytes 3063808 | tf_op jit(solution)/shard_map/all_gather | solution.py:160
  272.8 320.4 %reduce-scatter.2.cloned.1.call-start = ((), (), s32[]{:S(2)}) async-start(), calls=%async_computation.7 | async-start | bytes 3538944 | tf_op jit(solution)/shard_map/reduce_scatter | solution.py:163
  499.3 93.9 %copy-start.1 = (bf16[96,2048]{1,0:T(8,128)(2,1)S(1)}, bf16[96,2048]{1,0:T(8,128)(2,1)}, u32[]{:S(2)}) copy-start(bf16[96,2048]{1,0:T(8,128)(2,1)} %add_convert_fusion.1) | copy-start | bytes 1179652
  499.3 96.4 %copy-start.5 = (f32[2048]{0:T(1024)S(1)}, f32[2048]{0:T(1024)}, u32[]{:S(2)}) copy-start(f32[2048]{0:T(1024)} %param.29) | copy-start | bytes 24580
  499.3 96.4 %copy-start.6 = (f32[2048]{0:T(1024)S(1)}, f32[2048]{0:T(1024)}, u32[]{:S(2)}) copy-start(f32[2048]{0:T(1024)} %param.28) | copy-start | bytes 24580
Sparse Core Ops, SparseCore 0:
  9.5 92.3 all-gather.4
  104.0 64.0 all-gather.8
  272.3 220.4 all-gather.6
  494.8 50.6 all-gather.10
  558.0 35.0 reduce-scatter.1
where the time goes:
time: 608 us; the launch traced here: 604 us
  waiting for transfers between devices  421 us (69%)
  local copies, waits for them, and re-layouts  95.9 us (16%)
  matrix products  30.1 us (5%)
  other arithmetic  20.1 us (3%)
  between operations  13.3 us (2%)
  starting transfers between devices  13.1 us (2%)
  loops' own time  11.1 us (2%)
    all_gather x1, waiting for transfers between devices, body(): gathered = lax.all_gather(normed, 'tp', axis=0, tiled=True)  220 us
    all_gather x2, waiting for transfers between devices, in_one_piece(): lax.all_gather(both, axis, axis=dim, tiled=True)  80.5 us
    all_gather x1, waiting for transfers between devices, body(): lax.all_gather(down_weight, 'sp', axis=1, tiled=True)  46.2 us
    all_to_all x1, waiting for transfers between devices, sum_at_owner(): lax.all_to_all(pieces, axis, split_axis=0, concat_axis=0, tiled=True)  38.2 us
    unnamed x17, local copies, waits for them, and re-layouts  37.4 us
    reduce_scatter x1, waiting for transfers between devices, body(): lax.psum_scatter(partial_terms.astype(jnp.bfloat16), 'tp', scatter_dimens...  35.3 us
    reshape x1, local copies, waits for them, and re-layouts, attend(): key_blocks = key_piece.reshape(blocks, block_len, head_count, head_dim)  18.8 us
    reshape x1, local copies, waits for them, and re-layouts, attend(): value_blocks = value_piece.reshape(blocks, block_len, head_count, head_dim)  18.8 us
  transfers between devices with their start and end apart: 7, of which 5 were waited for; matrix products, arithmetic and copies ran while one was open for 21% of the time, Pallas kernels for 0%

commit v1 on v0

--- a/solution.py
+++ b/solution.py
@@ -1,3 +1,4 @@
+import functools
 import jax
 import jax.numpy as jnp
 from jax import lax
@@ -5,6 +6,16 @@
 
 ALPHA = 8.0**0.25
 EPSILON = 1e-05
+
+
+def move_steps_all(frame_in, ax_name):
+    view_out = lax.axis_size(ax_name)
+    x_now = jnp.concatenate([frame_in] * view_out, 0)
+    then = lax.all_to_all(x_now, axis_name=ax_name, split_axis=0, concat_axis=0, tiled=True)
+    return then
+
+
+_name_tracks = functools.partial(move_steps_all, ax_name="tp")
 
 
 def laid_out(pieces, dim):
@@ -150,7 +161,7 @@
     normed = layer_norm(
         ALPHA * stream_own.astype(jnp.float32) + mix_out, mix_gain, mix_bias
     ).astype(jnp.bfloat16)
-    gathered = lax.all_gather(normed, "tp", axis=0, tiled=True)
+    gathered = _name_tracks(normed)
     pieces = in_one_piece((gate_weight, up_weight), "sp", 0, 1)
     gate_part = jnp.dot(gathered, pieces[0], preferred_element_type=jnp.float32)
     up_part = jnp.dot(gathered, pieces[1], preferred_element_type=jnp.float32)

time: 608 us -> 579 us (0.952)
  waiting for transfers between devices: 421 us -> 387 us
    all_gather x1 -> x0, waiting for transfers between devices: 220 us -> none  [body(): gathered = lax.all_gather(normed, 'tp', axis=0, tiled=True)]
    all_gather x1, waiting for transfers between devices: 46.2 us -> 153 us  [body(): lax.all_gather(down_weight, 'sp', axis=1, tiled=True)]
    reduce_scatter x1, waiting for transfers between devices: 35.3 us -> 76.1 us  [body(): lax.psum_scatter(partial_terms.astype(jnp.bfloat16), 'tp', scatter_dimens...]
    all_to_all x0 -> x1, waiting for transfers between devices: none -> 38.3 us  [move_steps_all(): lax.all_to_all(x_now, axis_name=ax_name, split_axis=0, concat_axis=0, til...]
    unnamed x17 -> x25, local copies, waits for them, and re-layouts: 37.4 us -> 38.2 us
  transfers between devices with their start and end apart: 7 -> 7, of which waited for: 5 -> 5; matrix products, arithmetic and copies ran while one was open for 21% -> 22% of each run, Pallas kernels for 0% -> 0%
where the time goes in v1:
time: 579 us; the launch traced here: 575 us
  waiting for transfers between devices  387 us (67%)
  local copies, waits for them, and re-layouts  96.5 us (17%)
  matrix products  30.1 us (5%)
  other arithmetic  19.3 us (3%)
  starting transfers between devices  17.4 us (3%)
  between operations  13.4 us (2%)
  loops' own time  10.9 us (2%)
    all_gather x1, waiting for transfers between devices, body(): lax.all_gather(down_weight, 'sp', axis=1, tiled=True)  153 us
    all_gather x2, waiting for transfers between devices, in_one_piece(): lax.all_gather(both, axis, axis=dim, tiled=True)  82.2 us
    reduce_scatter x1, waiting for transfers between devices, body(): lax.psum_scatter(partial_terms.astype(jnp.bfloat16), 'tp', scatter_dimens...  76.1 us
    all_to_all x1, waiting for transfers between devices, move_steps_all(): lax.all_to_all(x_now, axis_name=ax_name, split_axis=0, concat_axis=0, til...  38.3 us
    unnamed x25, local copies, waits for them, and re-layouts  38.2 us
    all_to_all x1, waiting for transfers between devices, sum_at_owner(): lax.all_to_all(pieces, axis, split_axis=0, concat_axis=0, tiled=True)  37.6 us
    reshape x1, local copies, waits for them, and re-layouts, attend(): key_blocks = key_piece.reshape(blocks, block_len, head_count, head_dim)  18.8 us
    reshape x1, local copies, waits for them, and re-layouts, attend(): value_blocks = value_piece.reshape(blocks, block_len, head_count, head_dim)  18.8 us
  transfers between devices with their start and end apart: 7, of which 5 were waited for; matrix products, arithmetic and copies ran while one was open for 22% of the time, Pallas kernels for 0%

profile of v1, /device:TPU:0, one launch (start us, length us, event | category | flops | bytes accessed | tf_op | source)
XLA Modules:
  0.0 574.9 jit_solution(18210850682517216798)
XLA Ops:
  6.5 2.2 pad_maximum_fusion
  8.8 1.8 pad_maximum_fusion.1
  10.6 0.7 broadcast_in_dim.56
  11.3 8.2 %all-to-all-start = ((f32[16,768,4]{1,2,0:T(4,128)}), f32[16,768,4]{1,2,0:T(4,128)S(1)}, u32[]{:S(2)}, u32[]{:S(2)}) async-start(f32[16,768,4]{1,2,0:T(4,128)} %broadcast_in_dim.56), calls=%async_computation | async-start | bytes 393216 | tf_op jit(solution)/shard_map/all_to_all | solution.py:29
  19.7 82.2 %all-gather.4.cloned.1.call-done = bf16[12288,512]{1,0:T(8,128)(2,1)} async-done(((bf16[768,512]{1,0:T(8,128)(2,1)}), bf16[12288,512]{1,0:T(8,128)(2,1)}) %all-gather.4.cloned.1.call-update) | async-done | bytes 12582928 | tf_op jit(solution)/shard_map/all_gather | solution.py:42
  101.9 10.1 %fusion.36 = (bf16[12288,256]{1,0:T(8,128)(2,1)}, bf16[12288,256]{1,0:T(8,128)(2,1)}) fusion(bf16[12288,512]{1,0:T(8,128)(2,1)} %all-gather.4.cloned.1.call-done), kind=kLoop, calls=%fused_computation.59 | loop fusion | bytes 25165824 | tf_op jit(solution)/shard_map/split | solution.py:42
  112.0 18.8 %reshape.84 = bf16[16,768,4,64]{3,2,1,0:T(4,128)(2,1)} reshape(bf16[12288,256]{1,0:T(8,128)(2,1)} %get-tuple-element.251) | data formatting | bytes 12582912 | tf_op jit(solution)/shard_map/reshape | solution.py:91
  130.8 18.1 %copy.20 = bf16[16,768,4,64]{1,3,2,0:T(8,128)(2,1)} copy(bf16[16,768,4,64]{3,2,1,0:T(4,128)(2,1)} %reshape.84) | data formatting | bytes 12582912
  148.9 18.8 %reshape.85 = bf16[16,768,4,64]{3,2,1,0:T(4,128)(2,1)} reshape(bf16[12288,256]{1,0:T(8,128)(2,1)} %get-tuple-element.250) | data formatting | bytes 12582912 | tf_op jit(solution)/shard_map/reshape | solution.py:92
  167.6 18.1 %copy.21 = bf16[16,768,4,64]{1,3,2,0:T(8,128)(2,1)} copy(bf16[16,768,4,64]{3,2,1,0:T(4,128)(2,1)} %reshape.85) | data formatting | bytes 12582912
  185.8 33.7 %while.15 = (s32[]{:T(128)}, f32[4,768]{1,0:T(4,128)S(1)}, f32[4,768]{1,0:T(4,128)S(1)}, f32[768,4,64]{0,2,1:T(8,128)S(1)}, s32[16]{0:T(128)S(1)}, /*index=5*/s3...) while((s32[]{:T(128)}, f32[4,768]{1,0:T(4,128)S(1)}, ...), condition=%wide.region_5.6_spmd.clone, body=%wide.region_0.5_spmd.clone.sunk | while | flops 649800192 | bytes 33738040 | solution.py:128
  187.1 13.1 %conditional.3 = ((f32[4,768]{1,0:T(4,128)S(1)}, f32[4,768]{1,0:T(4,128)S(1)}, f32[768,4,64]{0,2,1:T(8,128)S(1)})) conditional(s32[]{:T(128)} %convert_element_type.103, (f32[4,768]{1,0:T(4,128)S(1)}, f32[4,768]{1,0:T(4,128)S(1)}, f32[768,4,64]{0,2,1:T(8,128)S(1)}) %tuple.42, (s32[]{:T(128)}, s32[]{:T(128)}, bf16[16,768,4,64]{1,3,2,0:T(8,128)(2,1)}, ...), branch_computations={%region_1.1_spmd, %region_2.4_spmd} | conditional | flops 649800192 | bytes 33734700 | solution.py:126
  188.1 3.9 fusion.4
  192.0 4.6 fusion.11
  196.6 3.5 fusion.3
  219.6 2.7 convolution_convert_fusion.1
  222.3 4.4 all-to-all-start.1
  227.5 37.6 %all-to-all-done.1 = bf16[8,96,2048]{2,1,0:T(8,128)(2,1)} async-done(((bf16[8,96,2048]{2,1,0:T(8,128)(2,1)}), bf16[8,96,2048]{2,1,0:T(8,128)(2,1)}, u32[]{:S(2)}, u32[]{:S(2)}) %all-to-all-start.1) | async-done | bytes 3145760 | tf_op jit(solution)/shard_map/all_to_all | solution.py:52
  265.2 2.5 reduce_sum.59
  267.6 1.2 fusion.33
  268.9 1.3 multiply_reduce_fusion.1
  270.2 1.2 constant_dynamic-update-slice_fusion.7
  271.7 1.7 copy-done.1
  273.4 4.4 all-to-all-start.2
  277.9 38.3 %all-to-all-done.2 = bf16[8,96,2048]{2,1,0:T(8,128)(2,1)} async-done(((bf16[8,96,2048]{2,1,0:T(8,128)(2,1)}), bf16[8,96,2048]{2,1,0:T(8,128)(2,1)}, u32[]{:S(2)}, u32[]{:S(2)}) %all-to-all-start.2) | async-done | bytes 3145760 | tf_op jit(solution)/shard_map/all_to_all | solution.py:14
  316.2 6.5 %fusion.27 = f32[768,704]{0,1:T(8,128)} fusion(bf16[768,2048]{1,0:T(8,128)(2,1)} %bitcast.13, bf16[2048,1408]{0,1:T(8,128)(2,1)} %all-gather.6.cloned.1.call-done), kind=kOutput, calls=%fused_computation.31 | convolution fusion | flops 2214592512 | bytes 8192000 | tf_op jit(solution)/shard_map/dot_general | solution.py:166
  322.8 152.5 %all-gather.8.cloned.1.call-done = bf16[704,2048]{1,0:T(8,128)(2,1)} async-done(((bf16[704,128]{1,0:T(8,128)(2,1)}), bf16[704,2048]{1,0:T(8,128)(2,1)}) %all-gather.8.cloned.1.call-update) | async-done | bytes 2883600 | tf_op jit(solution)/shard_map/all_gather | solution.py:171
  475.3 12.4 %convolution_convert_fusion = bf16[768,2048]{1,0:T(8,128)(2,1)} fusion(bf16[704,2048]{1,0:T(8,128)(2,1)} %all-gather.8.cloned.1.call-done, f32[768,704]{0,1:T(8,128)} %fusion.27, bf16[768,2048]{1,0:T(8,128)(2,1)} %bitcast.13, bf16[2048,1408]{0,1:T(8,128)(2,1)} %all-gather.6.cloned.1.call-done), kind=kOutput, calls=%fused_computation.27 | convolution fusion | flops 4434001920 | bytes 14221312 | tf_op jit(solution)/shard_map/dot_general | solution.py:169
  487.7 76.1 %reduce-scatter.2.cloned.1.call-done = bf16[96,2048]{1,0:T(8,128)(2,1)} async-done(((bf16[768,2048]{1,0:T(8,128)(2,1)}), bf16[96,2048]{1,0:T(8,128)(2,1)}) %reduce-scatter.2.cloned.1.call-update) | async-done | bytes 393232 | tf_op jit(solution)/shard_map/reduce_scatter | solution.py:174
  563.9 1.2 fusion.34
  565.1 1.3 multiply_reduce_fusion
  566.4 2.0 add_convert_fusion
  (95 shorter events, 12.5 us)
Async XLA Ops:
  6.5 213.0 %copy-start = (bf16[256,2048]{1,0:T(8,128)(2,1)S(1)}, bf16[256,2048]{1,0:T(8,128)(2,1)}, u32[]{:S(2)}) copy-start(bf16[256,2048]{1,0:T(8,128)(2,1)} %param.22) | copy-start | bytes 3145732
  6.5 4.1 copy-start.2
  6.5 13.0 %copy-start.3 = (bf16[768,256]{1,0:T(8,128)(2,1)S(1)}, bf16[768,256]{1,0:T(8,128)(2,1)}, u32[]{:S(2)}) copy-start(bf16[768,256]{1,0:T(8,128)(2,1)} %param.17) | copy-start | bytes 1179652
  6.5 95.4 %all-gather.4.cloned.1.call-start = ((), (), s32[]{:S(2)}) async-start(), calls=%async_computation.4 | async-start | bytes 13369344 | tf_op jit(solution)/shard_map/all_gather | solution.py:42
  8.8 269.1 %all-gather.6.cloned.1.call-start = ((), (), s32[]{:S(2)}) async-start(), calls=%async_computation.5 | async-start | bytes 6127616 | tf_op jit(solution)/shard_map/all_gather | solution.py:42
  11.3 174.4 %all-to-all-start = ((f32[16,768,4]{1,2,0:T(4,128)}), f32[16,768,4]{1,2,0:T(4,128)S(1)}, u32[]{:S(2)}, u32[]{:S(2)}) async-start(f32[16,768,4]{1,2,0:T(4,128)} %broadcast_in_dim.56), calls=%async_computation | async-start | bytes 393216 | tf_op jit(solution)/shard_map/all_to_all | solution.py:29
  222.3 42.9 %all-to-all-start.1 = ((bf16[8,96,2048]{2,1,0:T(8,128)(2,1)}), bf16[8,96,2048]{2,1,0:T(8,128)(2,1)}, u32[]{:S(2)}, u32[]{:S(2)}) async-start(bf16[8,96,2048]{2,1,0:T(8,128)(2,1)} %bitcast.47), calls=%async_computation.1 | async-start | bytes 6291456 | tf_op jit(solution)/shard_map/all_to_all | solution.py:52
  226.7 43.4 %copy-start.4 = (f32[2048]{0:T(1024)S(1)}, f32[2048]{0:T(1024)}, u32[]{:S(2)}) copy-start(f32[2048]{0:T(1024)} %param.24) | copy-start | bytes 24580
  226.8 43.4 %copy-start.5 = (f32[2048]{0:T(1024)S(1)}, f32[2048]{0:T(1024)}, u32[]{:S(2)}) copy-start(f32[2048]{0:T(1024)} %param.23) | copy-start | bytes 24580
  226.8 248.5 %all-gather.8.cloned.1.call-start = ((), (), s32[]{:S(2)}) async-start(), calls=%async_computation.6 | async-start | bytes 3063808 | tf_op jit(solution)/shard_map/all_gather | solution.py:171
  271.7 1.7 copy-start.1
  273.4 42.9 %all-to-all-start.2 = ((bf16[8,96,2048]{2,1,0:T(8,128)(2,1)}), bf16[8,96,2048]{2,1,0:T(8,128)(2,1)}, u32[]{:S(2)}, u32[]{:S(2)}) async-start(bf16[8,96,2048]{2,1,0:T(8,128)(2,1)} %bitcast.48), calls=%async_computation.2 | async-start | bytes 6291456 | tf_op jit(solution)/shard_map/all_to_all | solution.py:14
  277.8 286.0 %reduce-scatter.2.cloned.1.call-start = ((), (), s32[]{:S(2)}) async-start(), calls=%async_computation.7 | async-start | bytes 3538944 | tf_op jit(solution)/shard_map/reduce_scatter | solution.py:174
  487.7 78.7 %copy-start.6 = (f32[2048]{0:T(1024)S(1)}, f32[2048]{0:T(1024)}, u32[]{:S(2)}) copy-start(f32[2048]{0:T(1024)} %param.29) | copy-start | bytes 24580
  487.7 78.7 %copy-start.7 = (f32[2048]{0:T(1024)S(1)}, f32[2048]{0:T(1024)}, u32[]{:S(2)}) copy-start(f32[2048]{0:T(1024)} %param.28) | copy-start | bytes 24580
Sparse Core Ops, SparseCore 0:
  9.5 92.3 all-gather.3
  104.0 64.0 all-gather.5
  229.7 245.5 all-gather.7
  487.9 75.9 reduce-scatter.1
